TPU v7x, 32 devices: a whole 2x2x4 slice. The times are simulated.
32 devices in a mesh: sp: 8 (over z, y), tp: 4 (over x, core).
Axes of the slice: x: 2, y: 2, z: 4, core: 2. Of those that a mesh axis runs over, the one named last changes fastest.
Arguments:
- queries: bfloat16 [8192, 1024], P('sp', 'tp'), may hold values from -6 to 6
- keys: bfloat16 [8192, 1024], P('sp', 'tp'), may hold values from -6 to 6
- values: bfloat16 [8192, 1024], P('sp', 'tp'), may hold values from -6 to 6
- stick_bias: bfloat16 [8192, 8], P('sp', 'tp'), may hold values from -14 to 0
- residual: bfloat16 [8192, 2048], P(('sp', 'tp')), may hold values from -6 to 6
- out_weight: bfloat16 [1024, 2048], replicated, may hold values from -0.1875 to 0.1875
- norm_gain: float32 [2048], replicated, may hold values from 0.1 to 1.9
- gate_weight: bfloat16 [2048, 5632], P('sp', 'tp'), may hold values from -0.125 to 0.125
- value_weight: bfloat16 [2048, 5632], P('sp', 'tp'), may hold values from -0.125 to 0.125
- down_weight: bfloat16 [2048, 5632], P('sp', 'tp'), may hold values from -0.078125 to 0.078125
- conv_gate: float32 [3, 5632], P(None, 'tp'), may hold values from -3.5 to 3.5
- conv_value: float32 [3, 5632], P(None, 'tp'), may hold values from -3.5 to 3.5
Outputs:
- mixed: bfloat16 [8192, 2048], P(('sp', 'tp'))
All inputs are finite; a program needn't handle non-finite values.
Results may differ from a plain program's by a relative error of at most 0.023.
Values may be sent and summed in bfloat16 or wider, within the bound.
A program may use at most 128 MiB of HBM per device.

v0:
```python
import jax
import jax.numpy as jnp
from jax import lax
from jax.sharding import PartitionSpec as P

EPS = 1e-06


def from_behind(block, axis, distance):
    devices = range(lax.axis_size(axis))
    route = [(i - distance, i) for i in devices if i - distance in devices]
    return lax.ppermute(block, axis, route)


def round_keep(value):
    return lax.optimization_barrier(value.astype(jnp.bfloat16)).astype(jnp.float32)


def local(
    queries,
    keys,
    values,
    stick_bias,
    residual,
    out_weight,
    norm_gain,
    gate_weight,
    value_weight,
    down_weight,
    conv_gate,
    conv_value,
):
    rows_here = queries.shape[0]
    heads_here = stick_bias.shape[1]
    head_size = queries.shape[1] // heads_here
    width_here = queries.shape[1]
    model_width = residual.shape[1]
    sp_count = lax.axis_size("sp")
    tp_count = lax.axis_size("tp")
    my_block = lax.axis_index("sp")
    row_share = rows_here // tp_count
    scale = head_size ** (-0.5)
    key_all, value_all, bias_all = (
        lax.all_gather(keys, "sp", axis=0, tiled=True),
        lax.all_gather(values, "sp", axis=0, tiled=True),
        lax.all_gather(stick_bias, "sp", axis=0, tiled=True),
    )
    query_heads = queries.reshape(rows_here, heads_here, head_size)
    query_pos = my_block * rows_here + jnp.arange(rows_here, dtype=jnp.int32)

    def visit(step, carry):
        block_index = my_block - step

        def work(state):
            acc_out, acc_log = state
            offset = block_index * rows_here
            key_block = lax.dynamic_slice_in_dim(key_all, offset, rows_here, 0).reshape(
                rows_here, heads_here, head_size
            )
            value_block = lax.dynamic_slice_in_dim(value_all, offset, rows_here, 0).reshape(
                rows_here, heads_here, head_size
            )
            bias_block = lax.dynamic_slice_in_dim(bias_all, offset, rows_here, 0).astype(
                jnp.float32
            )
            scores = (
                jnp.einsum(
                    "qhd,khd->hqk", query_heads, key_block, preferred_element_type=jnp.float32
                )
                * scale
            )
            scores = scores + bias_block.T[:, None, :]
            key_pos = offset + jnp.arange(rows_here, dtype=jnp.int32)
            before = (key_pos[None, :] < query_pos[:, None])[None]
            log_keep = jnp.where(before, jax.nn.log_sigmoid(-scores), 0.0)
            after = lax.cumsum(log_keep, axis=2, reverse=True) - log_keep
            stick = jnp.where(
                before, jnp.exp(jax.nn.log_sigmoid(scores) + after + acc_log[:, :, None]), 0.0
            )
            stick = stick.astype(jnp.bfloat16)
            acc_out = acc_out + jnp.einsum(
                "hqk,khd->qhd", stick, value_block, preferred_element_type=jnp.float32
            )
            acc_log = acc_log + jnp.sum(log_keep, axis=2)
            return (acc_out, acc_log)

        return lax.cond(block_index >= 0, work, lambda state: state, carry)

    start_state = (
        jnp.zeros((rows_here, heads_here, head_size), jnp.float32),
        jnp.zeros((heads_here, rows_here), jnp.float32),
    )
    acc_out, acc_log = lax.fori_loop(0, sp_count, visit, start_state)
    attended = acc_out.reshape(rows_here, width_here).astype(jnp.bfloat16)
    row_heads = lax.all_to_all(attended, "tp", split_axis=0, concat_axis=1, tiled=True)
    grouped = jnp.einsum(
        "rgc,gcd->grd",
        row_heads.reshape(row_share, tp_count, width_here),
        out_weight.reshape(tp_count, width_here, model_width),
        preferred_element_type=jnp.float32,
    )
    projected = jnp.sum(round_keep(grouped), axis=0)
    middle_f = (residual.astype(jnp.float32) + projected).astype(jnp.bfloat16).astype(jnp.float32)
    normed = (
        middle_f
        * lax.rsqrt(jnp.mean(middle_f * middle_f, axis=-1, keepdims=True) + EPS)
        * norm_gain
    ).astype(jnp.bfloat16)
    normed_all = lax.all_gather(normed, "tp", axis=0, tiled=True)
    gate_sum = jnp.dot(
        normed_all,
        lax.all_gather(gate_weight, "sp", axis=0, tiled=True),
        preferred_element_type=jnp.float32,
    )
    value_sum = jnp.dot(
        normed_all,
        lax.all_gather(value_weight, "sp", axis=0, tiled=True),
        preferred_element_type=jnp.float32,
    )
    gate_up = gate_sum.astype(jnp.bfloat16)
    value_up = value_sum.astype(jnp.bfloat16)
    rim_gate, rim_value = from_behind((gate_up[-2:], value_up[-2:]), "sp", 1)

    def depthwise(rim, upward, taps):
        extended = jnp.concatenate([rim, upward], axis=0).astype(jnp.float32)
        return taps[0] * extended[:-2] + taps[1] * extended[1:-1] + taps[2] * extended[2:]

    hidden = (
        jax.nn.silu(depthwise(rim_gate, gate_up, conv_gate))
        * depthwise(rim_value, value_up, conv_value)
    ).astype(jnp.bfloat16)
    terms = lax.dot_general(
        hidden,
        lax.all_gather(down_weight, "sp", axis=0, tiled=True),
        (((1,), (1,)), ((), ())),
        preferred_element_type=jnp.float32,
    )
    down_total = lax.psum_scatter(
        round_keep(terms).astype(jnp.bfloat16), "tp", scatter_dimension=0, tiled=True
    ).astype(jnp.float32)
    return (middle_f + down_total).astype(jnp.bfloat16)


def solution(mesh):
    in_specs = (
        P("sp", "tp"),
        P("sp", "tp"),
        P("sp", "tp"),
        P("sp", "tp"),
        P(("sp", "tp"), None),
        P(),
        P(),
        P("sp", "tp"),
        P("sp", "tp"),
        P("sp", "tp"),
        P(None, "tp"),
        P(None, "tp"),
    )
    out_specs = P(("sp", "tp"), None)
    return jax.shard_map(local, mesh=mesh, in_specs=in_specs, out_specs=out_specs, check_vma=False)
```

profile of v0, /device:TPU:0, one launch (start us, length us, event | category | flops | bytes accessed | tf_op | source)
XLA Modules:
  0.0 1038.3 jit_solution(2334887886741834532)
XLA Ops:
  6.5 2.1 copy.22
  8.6 0.0 all-gather.7.cloned.1.call-update
  8.6 0.0 all-gather.9.cloned.1.call-start
  8.7 2.0 copy.23
  10.7 0.0 all-gather.9.cloned.1.call-update
  10.7 0.0 all-gather.15.cloned.1.call-start
  10.8 0.7 all-gather.15.cloned.1.call-update
  11.5 0.0 all-gather.11.cloned.1.call-start
  11.5 1.2 copy.24
  12.8 0.3 copy.25
  13.1 33.0 %all_gather.23 = bf16[8192,2]{0,1:T(2,128)(2,1)S(1)} all-gather(bf16[1024,2]{0,1:T(2,128)(2,1)S(1)} %copy-done.7), channel_id=1, replica_groups=mesh['sp'=8,'tp'=4] {'sp'}, dimensions={0}, use_global_device_ids=true | all-gather | bytes 36864 | tf_op jit(solution)/shard_map/all_gather | solution.py:46
  46.1 39.2 %all-gather.7.cloned.1.call-done = bf16[8192,256]{0,1:T(8,128)(2,1)} async-done(((bf16[1024,256]{0,1:T(8,128)(2,1)}), bf16[8192,256]{0,1:T(8,128)(2,1)}) %all-gather.7.cloned.1.call-update) | async-done | bytes 4194320 | tf_op jit(solution)/shard_map/all_gather | solution.py:45
  85.2 73.5 %all-gather.9.cloned.1.call-done = bf16[8192,256]{0,1:T(8,128)(2,1)} async-done(((bf16[1024,256]{0,1:T(8,128)(2,1)}), bf16[8192,256]{0,1:T(8,128)(2,1)}) %all-gather.9.cloned.1.call-update) | async-done | bytes 4194320 | tf_op jit(solution)/shard_map/all_gather | solution.py:44
  158.8 0.1 broadcast_in_dim.27
  158.9 89.2 %while.16 = (s32[]{:T(128)}, f32[1024,2,128]{0,2,1:T(8,128)S(1)}, f32[2,1024]{1,0:T(2,128)S(1)}, s32[]{:T(128)}, bf16[8192,256]{0,1:T(8,128)(2,1)}, /*index=5*/b...) while((s32[]{:T(128)}, f32[1024,2,128]{0,2,1:T(8,128)S(1)}, ...), condition=%wide.region_6.7_spmd.clone, body=%wide.region_0.6_spmd.clone.sunk | while | flops 1414924288 | bytes 135303536 | solution.py:93
  159.2 66.4 %conditional.3 = ((f32[1024,2,128]{0,2,1:T(8,128)S(1)}, f32[2,1024]{1,0:T(2,128)S(1)})) conditional(s32[]{:T(128)} %convert_element_type.108, (f32[1024,2,128]{0,2,1:T(8,128)S(1)}, f32[2,1024]{1,0:T(2,128)S(1)}) %tuple.55, (s32[]{:T(128)}, bf16[8192,256]{0,1:T(8,128)(2,1)}, s32[]{:T(128)}, bf16[8192,256]{0,1:T(8,128)(2,1)}, ...), branch_computations={%region_1.0_spmd, %region_2.5_spmd} | conditional | flops 1414924288 | bytes 135299200 | solution.py:87
  159.3 1.3 constant_dynamic-slice_fusion
  160.6 0.7 broadcast_compare_fusion
  161.2 10.8 %fusion.17 = (f32[2,1024]{1,0:T(2,128)S(1)}, f32[2,1024,1024]{1,2,0:T(8,128)}, f32[2,1024,1024]{2,1,0:T(8,128)}) fusion(f32[2,1024]{1,0:T(2,128)S(1)} %convert_bitcast_fusion, pred[1024,1024]{0,1:T(8,128)(4,1)S(1)} %broadcast_compare_fusion, bf16[1024,2,128]{0,2,1:T(8,128)(2,1)S(1)} %bitcast.57, bf16[1024,2,128]{2,0,1:T(8,128)(2,1)S(1)} %get-tuple-element.177), kind=kOutput, calls=%fused_computation.32 | convolution fusion | flops 559937536 | bytes 18890752 | tf_op jit(solution)/shard_map/while/body/eval_jaxpr/cond/branch_1_fun/qhd,khd->hqk/dot_general | solution.py:67
  172.1 24.5 %fusion.14 = f32[2,1024,8,128]{1,2,3,0:T(8,128)S(1)} fusion(f32[2,1024,8,128]{1,3,2,0:T(8,128)} %bitcast.55), kind=kOutput, calls=%fused_computation.19 | output fusion | flops 266338304 | bytes 16777216 | tf_op jit(solution)/shard_map/reduce-window
  196.6 3.3 copy-done
  199.8 0.1 reduce-window.5
  200.0 4.6 broadcast_add_fusion
  204.6 5.0 copy.20
  209.6 14.9 %fusion.7 = bf16[2,1024,1024]{1,2,0:T(8,128)(2,1)S(1)} fusion(f32[2,1024,8,128]{1,3,2,0:T(8,128)S(1)} %copy.20, f32[2,1024,1024]{2,1,0:T(8,128)} %get-tuple-element.257, f32[2,1024]{1,0:T(2,128)S(1)} %get-tuple-element.179, f32[2,1024]{1,0:T(2,128)S(1)} %convert_bitcast_fusion, pred[1024,1024]{0,1:T(8,128)(4,1)S(1)} %broadcast_compare_fusion), kind=kLoop, calls=%fused_computation.8 | loop fusion | flops 48234496 | bytes 22036480 | tf_op jit(solution)/shard_map/while/body/eval_jaxpr/cond/branch_1_fun/convert_element_type | solution.py:80
  224.5 0.9 fusion.16
  229.5 8.5 conditional.3
  238.3 0.2 conditional.3
  238.8 0.2 conditional.3
  239.2 0.2 conditional.3
  239.7 0.2 conditional.3
  240.1 0.2 conditional.3
  240.6 0.2 conditional.3
  248.1 0.1 convert_element_type.63
  248.1 0.4 reshape.73
  248.5 0.3 copy.29
  248.9 11.5 %all_to_all.13 = bf16[4,256,256]{2,1,0:T(8,128)(2,1)S(1)} all-to-all(bf16[4,256,256]{2,1,0:T(8,128)(2,1)S(1)} %copy.29), channel_id=1, replica_groups=mesh['sp'=8,'tp'=4] {'tp'}, dimensions={0} | all-to-all | bytes 1048576 | tf_op jit(solution)/shard_map/all_to_all | solution.py:95
  260.4 3.4 convolution_convert_fusion.3
  263.8 0.8 convert_reduce_fusion
  264.6 0.4 copy-done.3
  265.0 0.4 fusion.25
  265.4 1.3 fusion.27
  266.7 0.0 all-gather.11.cloned.1.call-update
  266.8 0.0 all-gather.13.cloned.1.call-start
  266.8 0.5 all-gather.13.cloned.1.call-update
  267.3 0.0 all-gather.17.cloned.1.call-start
  267.4 0.5 all-gather.17.cloned.1.call-update
  267.9 0.0 reduce-scatter.2.cloned.1.call-start
  268.0 0.1 slice_reduce_fusion.2
  268.1 0.0 all-gather.15.cloned.1.call-done
  268.1 507.7 %all-gather.11.cloned.1.call-done = bf16[1024,2048]{1,0:T(8,128)(2,1)} async-done(((bf16[256,2048]{1,0:T(8,128)(2,1)}), bf16[1024,2048]{1,0:T(8,128)(2,1)}) %all-gather.11.cloned.1.call-update) | async-done | bytes 4194320 | tf_op jit(solution)/shard_map/all_gather | solution.py:109
  775.8 10.1 convolution_convert_fusion
  785.9 1.6 copy-done.1
  787.5 3.4 collective-permute-start.1
  790.9 79.4 %all-gather.13.cloned.1.call-done = bf16[2048,1408]{1,0:T(8,128)(2,1)} async-done(((bf16[256,1408]{1,0:T(8,128)(2,1)}), bf16[2048,1408]{1,0:T(8,128)(2,1)}) %all-gather.13.cloned.1.call-update) | async-done | bytes 5767184 | tf_op jit(solution)/shard_map/all_gather | solution.py:112
  870.3 10.3 convolution_convert_fusion.1
  880.6 2.5 collective-permute-start
  883.1 3.1 maximum_convert_fusion.1
  886.1 3.1 maximum_convert_fusion
  889.2 73.7 %all-gather.17.cloned.1.call-done = bf16[2048,1408]{1,0:T(8,128)(2,1)} async-done(((bf16[256,1408]{1,0:T(8,128)(2,1)}), bf16[2048,1408]{1,0:T(8,128)(2,1)}) %all-gather.17.cloned.1.call-update) | async-done | bytes 5767184 | tf_op jit(solution)/shard_map/all_gather | solution.py:134
  963.0 22.6 %convolution_convert_fusion.2 = bf16[1024,2048]{1,0:T(8,128)(2,1)} fusion(bf16[2048,1408]{1,0:T(8,128)(2,1)} %all-gather.17.cloned.1.call-done, f32[1026,1408]{1,0:T(8,128)} %maximum_convert_fusion.1, f32[1026,1408]{1,0:T(8,128)} %maximum_convert_fusion, f32[1408]{0:T(1024)S(1)} %get-tuple-element.233, f32[1408]{0:T(1024)S(1)} %get-tuple-element.234, ...), kind=kOutput, calls=%fused_computation.48 | convolution fusion | flops 5930745856 | bytes 44598272 | tf_op jit(solution)/shard_map/dot_general | solution.py:132
  985.6 0.0 reduce-scatter.2.cloned.1.call-update
  985.6 43.0 %reduce-scatter.2.cloned.1.call-done = bf16[256,2048]{1,0:T(8,128)(2,1)} async-done(((bf16[1024,2048]{1,0:T(8,128)(2,1)}), bf16[256,2048]{1,0:T(8,128)(2,1)}) %reduce-scatter.2.cloned.1.call-update) | async-done | bytes 1048592 | tf_op jit(solution)/shard_map/reduce_scatter | solution.py:138
  1028.7 2.6 fusion.28
  (33 shorter events, 0.1 us)
Async XLA Ops:
  6.5 6.5 copy-start.7
  6.5 78.7 %all-gather.7.cloned.1.call-start = ((), (), s32[]{:S(2)}) async-start(), calls=%async_computation.2 | async-start | bytes 4718592 | tf_op jit(solution)/shard_map/all_gather | solution.py:45
  8.6 150.2 %all-gather.9.cloned.1.call-start = ((), (), s32[]{:S(2)}) async-start(), calls=%async_computation.3 | async-start | bytes 4718592 | tf_op jit(solution)/shard_map/all_gather | solution.py:44
  10.7 257.4 %all-gather.15.cloned.1.call-start = ((), (), s32[]{:S(2)}) async-start(), calls=%async_computation.6 | async-start | bytes 6488064 | tf_op jit(solution)/shard_map/all_gather | solution.py:117
  11.5 764.3 %all-gather.11.cloned.1.call-start = ((), (), s32[]{:S(2)}) async-start(), calls=%async_computation.4 | async-start | bytes 5242880 | tf_op jit(solution)/shard_map/all_gather | solution.py:109
  196.6 3.3 copy-start
  263.8 1.2 copy-start.3
  263.8 1.6 copy-start.6
  265.0 2.9 copy-start.4
  265.0 2.9 copy-start.5
  266.8 603.5 %all-gather.13.cloned.1.call-start = ((), (), s32[]{:S(2)}) async-start(), calls=%async_computation.5 | async-start | bytes 6488064 | tf_op jit(solution)/shard_map/all_gather | solution.py:112
  267.3 695.6 %all-gather.17.cloned.1.call-start = ((), (), s32[]{:S(2)}) async-start(), calls=%async_computation.7 | async-start | bytes 6488064 | tf_op jit(solution)/shard_map/all_gather | solution.py:134
  267.9 760.7 %reduce-scatter.2.cloned.1.call-start = ((), (), s32[]{:S(2)}) async-start(), calls=%async_computation.8 | async-start | bytes 5242880 | tf_op jit(solution)/shard_map/reduce_scatter | solution.py:138
  785.9 1.6 copy-start.1
  787.5 95.5 %collective-permute-start.1 = (bf16[2,1408]{1,0:T(2,128)(2,1)S(1)}, bf16[2,1408]{1,0:T(2,128)(2,1)S(1)}, u32[]{:S(2)}, u32[]{:S(2)}) collective-permute-start(bf16[2,1408]{1,0:T(2,128)(2,1)S(1)} %slice.68), channel_id=1, source_target_pairs={{0,4},{4,8},{8,12},{12,16},{16,20},{20,24},{24,28},{1,5},{5,9},{9,... | collective-permute-start | bytes 16904 | tf_op jit(solution)/shard_map/ppermute | solution.py:12
  870.3 12.8 %copy-start.2 = (bf16[1024,1408]{1,0:T(8,128)(2,1)S(1)}, bf16[1024,1408]{1,0:T(8,128)(2,1)}, u32[]{:S(2)}) copy-start(bf16[1024,1408]{1,0:T(8,128)(2,1)} %copy-done.1) | copy-start | bytes 8650756
  880.6 5.5 collective-permute-start
Sparse Core Ops, SparseCore 0:
  9.5 75.6 all-gather.6
  87.4 71.2 all-gather.8
  161.0 90.8 all-gather.14
  266.9 508.8 all-gather.10
  777.8 92.4 all-gather.12
  872.3 90.5 all-gather.16
  985.7 42.8 reduce-scatter.1
where the time goes:
time: 1040 us
  waiting for transfers between devices  818 us (79%)
  matrix products  58.2 us (6%)
  other arithmetic  56.1 us (5%)
  blocking collectives  44.5 us (4%)
  loops' own time  23 us (2%)
  local copies, waits for them, and re-layouts  18.1 us (2%)
  between operations  13.9 us (1%)
    all_gather x1, waiting for transfers between devices, local(): normed_all = lax.all_gather(normed, 'tp', axis=0, tiled=True)  508 us
    all_gather x1, waiting for transfers between devices, local(): lax.all_gather(gate_weight, 'sp', axis=0, tiled=True)  79.4 us
    all_gather x1, waiting for transfers between devices, local(): lax.all_gather(down_weight, 'sp', axis=0, tiled=True)  73.7 us
    all_gather x1, waiting for transfers between devices, local(): lax.all_gather(keys, 'sp', axis=0, tiled=True)  73.5 us
    reduce_scatter x1, waiting for transfers between devices, local(): lax.psum_scatter(round_keep(terms).astype(jnp.bfloat16), 'tp', scatter_di...  43 us
    all_gather x1, waiting for transfers between devices, local(): lax.all_gather(values, 'sp', axis=0, tiled=True)  39.2 us
    all_gather x1, blocking collectives, local(): lax.all_gather(stick_bias, 'sp', axis=0, tiled=True)  33 us
    another operation x2, other arithmetic  24.6 us
  transfers between devices with their start and end apart: 9, of which 6 were waited for; matrix products, arithmetic and copies ran while one was open for 10% of the time, Pallas kernels for 0%

commit v1 on v0

--- a/solution.py
+++ b/solution.py
@@ -106,7 +106,12 @@
         * lax.rsqrt(jnp.mean(middle_f * middle_f, axis=-1, keepdims=True) + EPS)
         * norm_gain
     ).astype(jnp.bfloat16)
-    normed_all = lax.all_gather(normed, "tp", axis=0, tiled=True)
+    ring = [normed]
+    for hop in range(3):
+        ring.append(lax.ppermute(ring[-1], "tp", [(dev, (dev + 1) % 4) for dev in range(4)]))
+    normed_all = jnp.roll(
+        jnp.concatenate(ring[::-1], axis=0), (lax.axis_index("tp") + 1) * ring[0].shape[0], axis=0
+    )
     gate_sum = jnp.dot(
         normed_all,
         lax.all_gather(gate_weight, "sp", axis=0, tiled=True),

time: 1040 us -> 928 us (0.89)
  waiting for transfers between devices: 818 us -> 554 us
  starting transfers between devices: 6.08 us -> 141 us
    all_gather x1 -> x0, waiting for transfers between devices: 508 us -> none  [local(): normed_all = lax.all_gather(normed, 'tp', axis=0, tiled=True)]
    all_gather x1, waiting for transfers between devices: 73.7 us -> 355 us  [local(): lax.all_gather(down_weight, 'sp', axis=0, tiled=True)]
    ppermute x2, starting transfers between devices: 5.83 us -> 141 us  [from_behind(): return lax.ppermute(block, axis, route)]
    all_gather x1, waiting for transfers between devices: 79.4 us -> 0.02 us  [local(): lax.all_gather(gate_weight, 'sp', axis=0, tiled=True)]
    ppermute x0 -> x3, waiting for transfers between devices: none -> 42.6 us  [local(): lax.ppermute(ring[-1], 'tp', [(dev, (dev + 1) % 4) for dev in range(4)])]
  transfers between devices with their start and end apart: 9 -> 11, of which waited for: 6 -> 7; matrix products, arithmetic and copies ran while one was open for 10% -> 12% of each run, Pallas kernels for 0% -> 0%
where the time goes in v1:
time: 928 us; the launch traced here: 925 us
  waiting for transfers between devices  554 us (60%)
  starting transfers between devices  141 us (15%)
  matrix products  58.9 us (6%)
  other arithmetic  57.3 us (6%)
  blocking collectives  44.7 us (5%)
  loops' own time  27.9 us (3%)
  local copies, waits for them, and re-layouts  27 us (3%)
  between operations  14.1 us (2%)
    all_gather x1, waiting for transfers between devices, local(): lax.all_gather(down_weight, 'sp', axis=0, tiled=True)  355 us
    ppermute x2, starting transfers between devices, from_behind(): return lax.ppermute(block, axis, route)  141 us
    all_gather x1, waiting for transfers between devices, local(): lax.all_gather(keys, 'sp', axis=0, tiled=True)  73.5 us
    reduce_scatter x1, waiting for transfers between devices, local(): lax.psum_scatter(round_keep(terms).astype(jnp.bfloat16), 'tp', scatter_di...  43.1 us
    ppermute x3, waiting for transfers between devices, local(): lax.ppermute(ring[-1], 'tp', [(dev, (dev + 1) % 4) for dev in range(4)])  42.6 us
    all_gather x1, waiting for transfers between devices, local(): lax.all_gather(values, 'sp', axis=0, tiled=True)  38.4 us
    all_gather x1, blocking collectives, local(): lax.all_gather(stick_bias, 'sp', axis=0, tiled=True)  33.2 us
    another operation x2, other arithmetic  24.2 us
  transfers between devices with their start and end apart: 11, of which 7 were waited for; matrix products, arithmetic and copies ran while one was open for 12% of the time, Pallas kernels for 0%

profile of v1, /device:TPU:0, one launch (start us, length us, event | category | flops | bytes accessed | tf_op | source)
XLA Modules:
  0.0 924.7 jit_solution(11849645840206056347)
XLA Ops:
  6.5 2.1 copy.22
  8.6 0.0 all-gather.8.cloned.1.call-start
  8.7 2.0 copy.23
  10.7 0.0 all-gather.12.cloned.1.call-start
  10.8 0.7 all-gather.12.cloned.1.call-update
  11.5 0.5 all-gather.10.cloned.1.call-update
  12.1 1.2 copy.24
  13.4 0.3 copy.25
  13.6 33.2 %all_gather.20 = bf16[8192,2]{0,1:T(2,128)(2,1)S(1)} all-gather(bf16[1024,2]{0,1:T(2,128)(2,1)S(1)} %copy-done.7), channel_id=1, replica_groups=mesh['sp'=8,'tp'=4] {'sp'}, dimensions={0}, use_global_device_ids=true | all-gather | bytes 36864 | tf_op jit(solution)/shard_map/all_gather | solution.py:46
  46.8 38.4 %all-gather.6.cloned.1.call-done = bf16[8192,256]{0,1:T(8,128)(2,1)} async-done(((bf16[1024,256]{0,1:T(8,128)(2,1)}), bf16[8192,256]{0,1:T(8,128)(2,1)}) %all-gather.6.cloned.1.call-update) | async-done | bytes 4194320 | tf_op jit(solution)/shard_map/all_gather | solution.py:45
  85.3 73.5 %all-gather.8.cloned.1.call-done = bf16[8192,256]{0,1:T(8,128)(2,1)} async-done(((bf16[1024,256]{0,1:T(8,128)(2,1)}), bf16[8192,256]{0,1:T(8,128)(2,1)}) %all-gather.8.cloned.1.call-update) | async-done | bytes 4194320 | tf_op jit(solution)/shard_map/all_gather | solution.py:44
  158.8 0.1 broadcast_in_dim.27
  158.9 93.9 %while.16 = (s32[]{:T(128)}, f32[1024,2,128]{0,2,1:T(8,128)S(1)}, f32[2,1024]{1,0:T(2,128)S(1)}, s32[]{:T(128)}, bf16[8192,256]{0,1:T(8,128)(2,1)}, /*index=5*/b...) while((s32[]{:T(128)}, f32[1024,2,128]{0,2,1:T(8,128)S(1)}, ...), condition=%wide.region_6.7_spmd.clone, body=%wide.region_0.6_spmd.clone.sunk | while | flops 1414924288 | bytes 135303536 | solution.py:93
  159.3 66.3 %conditional.3 = ((f32[1024,2,128]{0,2,1:T(8,128)S(1)}, f32[2,1024]{1,0:T(2,128)S(1)})) conditional(s32[]{:T(128)} %convert_element_type.116, (f32[1024,2,128]{0,2,1:T(8,128)S(1)}, f32[2,1024]{1,0:T(2,128)S(1)}) %tuple.55, (s32[]{:T(128)}, bf16[8192,256]{0,1:T(8,128)(2,1)}, s32[]{:T(128)}, bf16[8192,256]{0,1:T(8,128)(2,1)}, ...), branch_computations={%region_1.0_spmd, %region_2.5_spmd} | conditional | flops 1414924288 | bytes 135299200 | solution.py:87
  159.3 1.3 constant_dynamic-slice_fusion
  160.6 0.7 broadcast_compare_fusion
  161.3 11.1 %fusion.17 = (f32[2,1024]{1,0:T(2,128)S(1)}, f32[2,1024,1024]{1,2,0:T(8,128)}, f32[2,1024,1024]{2,1,0:T(8,128)}) fusion(f32[2,1024]{1,0:T(2,128)S(1)} %convert_bitcast_fusion, pred[1024,1024]{0,1:T(8,128)(4,1)S(1)} %broadcast_compare_fusion, bf16[1024,2,128]{0,2,1:T(8,128)(2,1)S(1)} %bitcast.55, bf16[1024,2,128]{2,0,1:T(8,128)(2,1)S(1)} %get-tuple-element.177), kind=kOutput, calls=%fused_computation.32 | convolution fusion | flops 559937536 | bytes 18890752 | tf_op jit(solution)/shard_map/while/body/eval_jaxpr/cond/branch_1_fun/qhd,khd->hqk/dot_general | solution.py:67
  172.4 24.1 %fusion.14 = f32[2,1024,8,128]{1,2,3,0:T(8,128)S(1)} fusion(f32[2,1024,8,128]{1,3,2,0:T(8,128)} %bitcast.53), kind=kOutput, calls=%fused_computation.19 | output fusion | flops 266338304 | bytes 16777216 | tf_op jit(solution)/shard_map/reduce-window
  196.5 3.2 copy-done
  199.7 0.1 reduce-window.5
  199.8 4.6 broadcast_add_fusion
  204.5 5.1 copy.20
  209.5 14.9 %fusion.7 = bf16[2,1024,1024]{1,2,0:T(8,128)(2,1)S(1)} fusion(f32[2,1024,8,128]{1,3,2,0:T(8,128)S(1)} %copy.20, f32[2,1024,1024]{2,1,0:T(8,128)} %get-tuple-element.257, f32[2,1024]{1,0:T(2,128)S(1)} %get-tuple-element.179, f32[2,1024]{1,0:T(2,128)S(1)} %convert_bitcast_fusion, pred[1024,1024]{0,1:T(8,128)(4,1)S(1)} %broadcast_compare_fusion), kind=kLoop, calls=%fused_computation.8 | loop fusion | flops 48234496 | bytes 22036480 | tf_op jit(solution)/shard_map/while/body/eval_jaxpr/cond/branch_1_fun/convert_element_type | solution.py:80
  224.4 0.9 fusion.16
  229.7 9.3 %conditional.3 = ((f32[1024,2,128]{0,2,1:T(8,128)S(1)}, f32[2,1024]{1,0:T(2,128)S(1)})) conditional(s32[]{:T(128)} %convert_element_type.116, (f32[1024,2,128]{0,2,1:T(8,128)S(1)}, f32[2,1024]{1,0:T(2,128)S(1)}) %tuple.55, (s32[]{:T(128)}, bf16[8192,256]{0,1:T(8,128)(2,1)}, s32[]{:T(128)}, bf16[8192,256]{0,1:T(8,128)(2,1)}, ...), branch_computations={%region_1.0_spmd, %region_2.5_spmd} | conditional | flops 1414924288 | bytes 135299200 | solution.py:87
  242.8 0.2 conditional.3
  243.2 0.2 conditional.3
  243.6 0.2 conditional.3
  244.0 0.2 conditional.3
  244.4 0.2 conditional.3
  244.8 0.2 conditional.3
  252.9 0.1 convert_element_type.63
  253.0 0.4 reshape.73
  253.3 0.3 copy.29
  253.7 11.6 %all_to_all.13 = bf16[4,256,256]{2,1,0:T(8,128)(2,1)S(1)} all-to-all(bf16[4,256,256]{2,1,0:T(8,128)(2,1)S(1)} %copy.29), channel_id=1, replica_groups=mesh['sp'=8,'tp'=4] {'tp'}, dimensions={0} | all-to-all | bytes 1048576 | tf_op jit(solution)/shard_map/all_to_all | solution.py:95
  265.2 3.5 convolution_convert_fusion.3
  268.8 0.8 convert_reduce_fusion
  269.6 0.4 copy-done.3
  269.9 0.4 fusion.27
  270.3 0.3 fusion.29
  270.7 0.1 collective-permute-start
  270.7 14.2 %collective-permute-done = bf16[256,2048]{1,0:T(8,128)(2,1)S(1)} collective-permute-done((bf16[256,2048]{1,0:T(8,128)(2,1)S(1)}, bf16[256,2048]{1,0:T(8,128)(2,1)S(1)}, u32[]{:S(2)}, u32[]{:S(2)}) %collective-permute-start) | collective-permute-done | bytes 1048608 | tf_op jit(solution)/shard_map/ppermute | solution.py:111
  285.0 14.1 %collective-permute-done.1 = bf16[256,2048]{1,0:T(8,128)(2,1)S(1)} collective-permute-done((bf16[256,2048]{1,0:T(8,128)(2,1)S(1)}, bf16[256,2048]{1,0:T(8,128)(2,1)S(1)}, u32[]{:S(2)}, u32[]{:S(2)}) %collective-permute-start.1) | collective-permute-done | bytes 1048608 | tf_op jit(solution)/shard_map/ppermute | solution.py:111
  299.2 0.1 slice_reduce_fusion.2
  299.3 14.2 %collective-permute-done.2 = bf16[256,2048]{1,0:T(8,128)(2,1)} collective-permute-done((bf16[256,2048]{1,0:T(8,128)(2,1)S(1)}, bf16[256,2048]{1,0:T(8,128)(2,1)}, u32[]{:S(2)}, u32[]{:S(2)}) %collective-permute-start.2) | collective-permute-done | bytes 1048608 | tf_op jit(solution)/shard_map/ppermute | solution.py:111
  313.5 2.3 constant_dynamic-update-slice_fusion.7
  315.8 1.1 constant_dynamic-update-slice_fusion.6
  316.9 1.1 constant_dynamic-update-slice_fusion.5
  317.9 1.3 constant_dynamic-update-slice_fusion.4
  319.2 2.3 constant_dynamic-update-slice_fusion.3
  321.5 1.1 constant_dynamic-update-slice_fusion.2
  322.6 1.1 constant_dynamic-update-slice_fusion.1
  323.7 1.3 constant_dynamic-update-slice_fusion
  325.0 10.4 %convolution_convert_fusion = bf16[1024,1408]{1,0:T(8,128)(2,1)S(1)} fusion(bf16[2048,1408]{1,0:T(8,128)(2,1)} %all-gather.12.cloned.1.call-done, bf16[2048,2048]{1,0:T(8,128)(2,1)} %constant_dynamic-update-slice_fusion, s32[]{:T(128)S(6)} %select_n.34), kind=kOutput, calls=%fused_computation.46 | convolution fusion | flops 5907021824 | bytes 12845060 | tf_op jit(solution)/shard_map/dot_general | solution.py:120
  335.3 1.6 copy-done.1
  336.9 67.0 %collective-permute-start.4 = (bf16[2,1408]{1,0:T(2,128)(2,1)S(1)}, bf16[2,1408]{1,0:T(2,128)(2,1)S(1)}, u32[]{:S(2)}, u32[]{:S(2)}) collective-permute-start(bf16[2,1408]{1,0:T(2,128)(2,1)S(1)} %slice.68), channel_id=1, source_target_pairs={{0,4},{4,8},{8,12},{12,16},{16,20},{20,24},{24,28},{1,5},{5,9},{9,... | collective-permute-start | bytes 16904 | tf_op jit(solution)/shard_map/ppermute | solution.py:12
  404.0 10.3 %convolution_convert_fusion.1 = bf16[1024,1408]{1,0:T(8,128)(2,1)S(1)} fusion(bf16[2048,1408]{1,0:T(8,128)(2,1)} %all-gather.10.cloned.1.call-done, bf16[2048,2048]{1,0:T(8,128)(2,1)} %constant_dynamic-update-slice_fusion, s32[]{:T(128)S(6)} %select_n.34), kind=kOutput, calls=%fused_computation.47 | convolution fusion | flops 5907021824 | bytes 12845060 | tf_op jit(solution)/shard_map/dot_general | solution.py:115
  414.3 73.7 %collective-permute-start.3 = (bf16[2,1408]{1,0:T(2,128)(2,1)S(1)}, bf16[2,1408]{1,0:T(2,128)(2,1)S(1)}, u32[]{:S(2)}, u32[]{:S(2)}) collective-permute-start(bf16[2,1408]{1,0:T(2,128)(2,1)S(1)} %slice.64), channel_id=1, source_target_pairs={{0,4},{4,8},{8,12},{12,16},{16,20},{20,24},{24,28},{1,5},{5,9},{9,... | collective-permute-start | bytes 16904 | tf_op jit(solution)/shard_map/ppermute | solution.py:12
  488.1 3.1 maximum_convert_fusion.1
  491.1 3.1 maximum_convert_fusion
  494.2 354.7 %all-gather.14.cloned.1.call-done = bf16[2048,1408]{1,0:T(8,128)(2,1)} async-done(((bf16[256,1408]{1,0:T(8,128)(2,1)}), bf16[2048,1408]{1,0:T(8,128)(2,1)}) %all-gather.14.cloned.1.call-update) | async-done | bytes 5767184 | tf_op jit(solution)/shard_map/all_gather | solution.py:139
  849.0 22.8 %convolution_convert_fusion.2 = bf16[1024,2048]{1,0:T(8,128)(2,1)} fusion(bf16[2048,1408]{1,0:T(8,128)(2,1)} %all-gather.14.cloned.1.call-done, f32[1026,1408]{1,0:T(8,128)} %maximum_convert_fusion.1, f32[1026,1408]{1,0:T(8,128)} %maximum_convert_fusion, f32[1408]{0:T(1024)S(1)} %get-tuple-element.233, f32[1408]{0:T(1024)S(1)} %get-tuple-element.234, ...), kind=kOutput, calls=%fused_computation.48 | convolution fusion | flops 5930745856 | bytes 44598272 | tf_op jit(solution)/shard_map/dot_general | solution.py:137
  871.8 43.1 %reduce-scatter.2.cloned.1.call-done = bf16[256,2048]{1,0:T(8,128)(2,1)} async-done(((bf16[1024,2048]{1,0:T(8,128)(2,1)}), bf16[256,2048]{1,0:T(8,128)(2,1)}) %reduce-scatter.2.cloned.1.call-update) | async-done | bytes 1048592 | tf_op jit(solution)/shard_map/reduce_scatter | solution.py:143
  914.9 2.6 fusion.30
  (44 shorter events, 0.4 us)
Async XLA Ops:
  6.5 7.1 copy-start.7
  6.5 78.7 %all-gather.6.cloned.1.call-start = ((), (), s32[]{:S(2)}) async-start(), calls=%async_computation.2 | async-start | bytes 4718592 | tf_op jit(solution)/shard_map/all_gather | solution.py:45
  8.6 150.2 %all-gather.8.cloned.1.call-start = ((), (), s32[]{:S(2)}) async-start(), calls=%async_computation.3 | async-start | bytes 4718592 | tf_op jit(solution)/shard_map/all_gather | solution.py:44
  10.7 314.2 %all-gather.12.cloned.1.call-start = ((), (), s32[]{:S(2)}) async-start(), calls=%async_computation.5 | async-start | bytes 6488064 | tf_op jit(solution)/shard_map/all_gather | solution.py:122
  11.5 392.5 %all-gather.10.cloned.1.call-start = ((), (), s32[]{:S(2)}) async-start(), calls=%async_computation.4 | async-start | bytes 6488064 | tf_op jit(solution)/shard_map/all_gather | solution.py:117
  12.1 836.9 %all-gather.14.cloned.1.call-start = ((), (), s32[]{:S(2)}) async-start(), calls=%async_computation.6 | async-start | bytes 6488064 | tf_op jit(solution)/shard_map/all_gather | solution.py:139
  196.5 3.2 copy-start
  268.7 1.2 copy-start.3
  268.7 1.6 copy-start.4
  268.7 30.4 %copy-start.5 = (f32[3,1408]{1,0:T(4,128)S(1)}, f32[3,1408]{1,0:T(4,128)}, u32[]{:S(2)}) copy-start(f32[3,1408]{1,0:T(4,128)} %param.27) | copy-start | bytes 50692
  268.7 30.4 %copy-start.6 = (f32[3,1408]{1,0:T(4,128)S(1)}, f32[3,1408]{1,0:T(4,128)}, u32[]{:S(2)}) copy-start(f32[3,1408]{1,0:T(4,128)} %param.26) | copy-start | bytes 50692
  270.7 14.3 %collective-permute-start = (bf16[256,2048]{1,0:T(8,128)(2,1)S(1)}, bf16[256,2048]{1,0:T(8,128)(2,1)S(1)}, u32[]{:S(2)}, u32[]{:S(2)}) collective-permute-start(bf16[256,2048]{1,0:T(8,128)(2,1)S(1)} %fusion.29), channel_id=1, source_target_pairs={{0,1},{1,2},{2,3},{3,0},{4,5},{5,6},{6,7},{7,4},{8,9},{9,10},{10,1... | collective-permute-start | bytes 3145736 | tf_op jit(solution)/shard_map/ppermute | solution.py:111
  284.9 14.2 %collective-permute-start.1 = (bf16[256,2048]{1,0:T(8,128)(2,1)S(1)}, bf16[256,2048]{1,0:T(8,128)(2,1)S(1)}, u32[]{:S(2)}, u32[]{:S(2)}) collective-permute-start(bf16[256,2048]{1,0:T(8,128)(2,1)S(1)} %collective-permute-done), channel_id=1, source_target_pairs={{0,1},{1,2},{2,3},{3,0},{4,5},{5,6},{6,7},{7,4},{8,9},{9,10},{10,1... | collective-permute-start | bytes 3145736 | tf_op jit(solution)/shard_map/ppermute | solution.py:111
  285.0 630.0 %reduce-scatter.2.cloned.1.call-start = ((), (), s32[]{:S(2)}) async-start(), calls=%async_computation.7 | async-start | bytes 5242880 | tf_op jit(solution)/shard_map/reduce_scatter | solution.py:143
  299.2 14.3 %collective-permute-start.2 = (bf16[256,2048]{1,0:T(8,128)(2,1)S(1)}, bf16[256,2048]{1,0:T(8,128)(2,1)}, u32[]{:S(2)}, u32[]{:S(2)}) collective-permute-start(bf16[256,2048]{1,0:T(8,128)(2,1)S(1)} %collective-permute-done.1), channel_id=1, source_target_pairs={{0,1},{1,2},{2,3},{3,0},{4,5},{5,6},{6,7},{7,4},{8,9},{9,10},{10,1... | collective-permute-start | bytes 3145736 | tf_op jit(solution)/shard_map/ppermute | solution.py:111
  335.3 1.6 copy-start.1
  336.9 151.1 %collective-permute-start.4 = (bf16[2,1408]{1,0:T(2,128)(2,1)S(1)}, bf16[2,1408]{1,0:T(2,128)(2,1)S(1)}, u32[]{:S(2)}, u32[]{:S(2)}) collective-permute-start(bf16[2,1408]{1,0:T(2,128)(2,1)S(1)} %slice.68), channel_id=1, source_target_pairs={{0,4},{4,8},{8,12},{12,16},{16,20},{20,24},{24,28},{1,5},{5,9},{9,... | collective-permute-start | bytes 16904 | tf_op jit(solution)/shard_map/ppermute | solution.py:12
  404.0 84.0 %copy-start.2 = (bf16[1024,1408]{1,0:T(8,128)(2,1)S(1)}, bf16[1024,1408]{1,0:T(8,128)(2,1)}, u32[]{:S(2)}) copy-start(bf16[1024,1408]{1,0:T(8,128)(2,1)} %copy-done.1) | copy-start | bytes 8650756
  414.3 76.8 %collective-permute-start.3 = (bf16[2,1408]{1,0:T(2,128)(2,1)S(1)}, bf16[2,1408]{1,0:T(2,128)(2,1)S(1)}, u32[]{:S(2)}, u32[]{:S(2)}) collective-permute-start(bf16[2,1408]{1,0:T(2,128)(2,1)S(1)} %slice.64), channel_id=1, source_target_pairs={{0,4},{4,8},{8,12},{12,16},{16,20},{20,24},{24,28},{1,5},{5,9},{9,... | collective-permute-start | bytes 16904 | tf_op jit(solution)/shard_map/ppermute | solution.py:12
Sparse Core Ops, SparseCore 0:
  9.5 75.7 all-gather.5
  87.5 71.2 all-gather.7
  161.0 90.8 all-gather.11
  253.9 90.5 all-gather.9
  346.6 502.3 all-gather.13
  871.9 42.9 reduce-scatter.1
